TPU v7x, 32 devices: a whole 2x2x4 slice. The times are simulated.
32 devices in a mesh: sp: 16 (over z, y, x), tp: 2 (over core).
Axes of the slice: x: 2, y: 2, z: 4, core: 2. Of those that a mesh axis runs over, the one named last changes fastest.
Arguments:
- resid: bfloat16 [8192, 2048], P('sp'), may hold values from -6 to 6
- queries: bfloat16 [8192, 2048], P('sp', 'tp'), may hold values from -6 to 6
- keys: bfloat16 [8192, 512], P('sp', 'tp'), may hold values from -6 to 6
- values: bfloat16 [8192, 512], P('sp', 'tp'), may hold values from -6 to 6
- documents: int32 [8192], P('sp'), may hold values from 0 to 7, never falling along the last dimension, each value on 1 to 2048 neighbouring positions
- q_gain: float32 [64], replicated, may hold values from 0.5 to 6.5
- k_gain: float32 [64], replicated, may hold values from 0.5 to 6.5
- sink: float32 [32], P('tp'), may hold values from -1 to 5
- w_out: bfloat16 [2048, 2048], P('tp'), may hold values from -0.5 to 0.5
- n_gain: float32 [2048], replicated, may hold values from 0.1 to 1.9
- w_up: bfloat16 [2048, 8192], P('sp', 'tp'), may hold values from -0.125 to 0.125
- w_down: bfloat16 [8192, 2048], P('tp', 'sp'), may hold values from -0.0625 to 0.0625
Outputs:
- layer_out: bfloat16 [8192, 2048], P('sp')
All inputs are finite; a program needn't handle non-finite values.
Results may differ from a plain program's by a relative error of at most 0.018.
The roundings to bfloat16 on the way count: a program that leaves them out, or rounds other values in their place, can miss the bound.
Values may be sent and summed in bfloat16 or wider, within the bound.
A program may use at most 128 MiB of HBM per device.

v0:
```python
import jax
import jax.numpy as jnp
from jax import lax
from jax.sharding import PartitionSpec as P

WINDOW = 128
EPS = 1e-06


def extended(x, sides, width):
    for axis, dim in sides:
        count, length = (lax.axis_size(axis), x.shape[dim])
        up = [(i, (i + 1) % count) for i in range(count - 1)]
        down = [(j, i) for i, j in up]
        last = lax.slice_in_dim(x, length - width, length, axis=dim)
        initial = lax.slice_in_dim(x, 0, width, axis=dim)
        before = lax.ppermute(last, axis, up)
        after = lax.ppermute(initial, axis, down)
        x = jnp.concatenate([before, x, after], axis=dim)
    return x


def rms_scale(field, gain):
    wide = field.astype(jnp.float32)
    return wide * lax.rsqrt(jnp.mean(wide * wide, axis=-1, keepdims=True) + EPS) * gain


def mixer_partial(normed, w_up, w_down):
    upward = jnp.dot(
        normed, lax.all_gather(w_up, "sp", axis=0, tiled=True), preferred_element_type=jnp.float32
    )
    active = jnp.square(jax.nn.relu(upward)).astype(jnp.bfloat16)
    return jnp.dot(
        active, lax.all_gather(w_down, "sp", axis=1, tiled=True), preferred_element_type=jnp.float32
    )


def shards(
    resid, queries, keys, values, documents, q_gain, k_gain, sink, w_out, n_gain, w_up, w_down
):
    rows = resid.shape[0]
    head_size = q_gain.shape[0]
    heads_here = sink.shape[0]
    kv_here = keys.shape[1] // head_size
    group = heads_here // kv_here
    qnorm = rms_scale(queries.reshape(rows, kv_here, group, head_size), q_gain).astype(jnp.bfloat16)
    knorm = rms_scale(keys.reshape(rows, kv_here, head_size), k_gain).astype(jnp.bfloat16)
    vheads = values.reshape(rows, kv_here, head_size)
    doc_here = documents.astype(jnp.bfloat16)
    near_keys, near_values, near_docs = (
        extended(knorm, (("sp", 0),), WINDOW),
        extended(vheads, (("sp", 0),), WINDOW),
        extended(doc_here, (("sp", 0),), WINDOW),
    )
    offset = lax.axis_index("sp") * rows
    total = rows * lax.axis_size("sp")
    query_pos = offset + jnp.arange(rows, dtype=jnp.int32)
    key_pos = offset - WINDOW + jnp.arange(rows + 2 * WINDOW, dtype=jnp.int32)
    distance = key_pos[None, :] - query_pos[:, None]
    allowed = (jnp.abs(distance) <= WINDOW) & (key_pos[None, :] >= 0) & (key_pos[None, :] < total)
    allowed = allowed & (near_docs[None, :] == doc_here[:, None])
    heads_all = heads_here * lax.axis_size("tp")
    first_head = (lax.axis_index("tp") * heads_here).astype(jnp.float32)
    slopes = jnp.exp2(
        -8.0 * (first_head + jnp.arange(heads_here, dtype=jnp.float32) + 1.0) / heads_all
    )
    slopes = slopes.reshape(kv_here, group)
    sink_f = sink.reshape(kv_here, group)
    scores = jnp.einsum(
        "rkgd,skd->kgrs", qnorm, near_keys, preferred_element_type=jnp.float32
    ) * head_size ** (-0.5)
    scores = scores - slopes[:, :, None, None] * jnp.abs(distance).astype(jnp.float32)[None, None]
    scores = jnp.where(allowed[None, None], scores, jnp.float32(-1e30))
    highest = jnp.maximum(jnp.max(scores, axis=-1), sink_f[:, :, None])
    weights = jnp.exp(scores - highest[..., None])
    denom = jnp.sum(weights, axis=-1) + jnp.exp(sink_f[:, :, None] - highest)
    summed = jnp.einsum(
        "kgrs,skd->rkgd",
        weights.astype(jnp.bfloat16),
        near_values,
        preferred_element_type=jnp.float32,
    )
    attended = (
        (summed / denom.transpose(2, 0, 1)[..., None])
        .astype(jnp.bfloat16)
        .reshape(rows, heads_here * head_size)
    )
    head_mix = lax.psum(
        jnp.dot(attended, w_out, preferred_element_type=jnp.float32).astype(jnp.bfloat16), "tp"
    ).astype(jnp.float32)
    middle = (resid.astype(jnp.float32) + head_mix).astype(jnp.bfloat16)
    normed = rms_scale(middle, n_gain).astype(jnp.bfloat16)
    partial_sum = mixer_partial(normed, w_up, w_down)
    unit_mix = lax.psum(partial_sum.astype(jnp.bfloat16), "tp").astype(jnp.float32)
    return (middle.astype(jnp.float32) + unit_mix).astype(jnp.bfloat16)


def solution(mesh):
    placed = (
        P("sp", None),
        P("sp", "tp"),
        P("sp", "tp"),
        P("sp", "tp"),
        P("sp"),
        P(),
        P(),
        P("tp"),
        P("tp", None),
        P(),
        P("sp", "tp"),
        P("tp", "sp"),
    )
    return jax.shard_map(
        shards, mesh=mesh, in_specs=placed, out_specs=P("sp", None), check_vma=False
    )
```

profile of v0, /device:TPU:0, one launch (start us, length us, event | category | flops | bytes accessed | tf_op | source)
XLA Modules:
  0.0 589.4 jit_solution(10305533719375993461)
XLA Ops:
  7.4 0.7 convert_element_type.69
  8.1 0.5 fusion.45
  8.6 5.4 collective-permute-start.2
  14.1 1.3 collective-permute-start.3
  15.4 1.1 copy.22
  16.5 0.8 multiply_convert_fusion.1
  17.3 0.7 fusion.44
  18.0 5.2 collective-permute-start.4
  23.1 1.3 collective-permute-start.5
  24.4 0.9 fusion.43
  25.4 5.2 collective-permute-start
  30.6 0.6 fusion.37
  31.2 1.5 copy.23
  33.0 0.6 add_rsqrt_fusion
  33.6 0.3 fusion.20
  34.1 0.7 max.24
  35.0 1.3 collective-permute-start.1
  36.3 0.7 pad_maximum_fusion
  37.0 1.8 fusion.24
  38.8 12.5 %fusion.3 = (f32[4,4,512]{2,1,0:T(4,128)S(1)}, f32[4,768,512,4]{2,1,3,0:T(8,128)}) fusion(f32[512,768]{0,1:T(8,128)S(1)} %fusion.20, f32[4,4]{1,0:T(4,128)S(1)} %multiply_exponential_fusion, pred[512,768]{0,1:T(8,128)(4,1)S(1)} %fusion.24, bf16[512,4,4,64]{0,3,2,1:T(8,128)(2,1)S(1)} %bitcast.50, f32[64]{0:T(128)} %param.17, f32[512,4,4]{0,2,1:T(4,128)} %add_rsqrt_fusion, ...), kind=kOutput, calls=%fused_computation.5 | convolution fusion | flops 840032256 | bytes 28639552 | tf_op jit(solution)/shard_map/rkgd,skd->kgrs/dot_general | solution.py:69
  51.3 12.1 %fusion.1 = f32[4,4,512]{2,1,0:T(4,128)S(1)} fusion(f32[4,768,512,4]{2,1,3,0:T(8,128)} %get-tuple-element.12, f32[4,4,512]{2,1,0:T(4,128)S(1)} %broadcast_maximum_fusion, f32[512,768]{0,1:T(8,128)S(1)} %fusion.20, f32[4,4]{1,0:T(4,128)S(1)} %multiply_exponential_fusion, pred[512,768]{0,1:T(8,128)(4,1)S(1)} %fusion.24), kind=kLoop, calls=%fused_computation.3 | loop fusion | flops 37740544 | bytes 27197504 | tf_op jit(solution)/shard_map/reduce_sum | solution.py:76
  63.5 12.5 %fusion.15 = bf16[512,4,4,64]{0,3,2,1:T(8,128)(2,1)S(1)} fusion(f32[4,768,512,4]{2,1,3,0:T(8,128)} %get-tuple-element.12, f32[4,4,512]{2,1,0:T(4,128)S(1)} %broadcast_maximum_fusion, f32[512,768]{0,1:T(8,128)S(1)} %fusion.20, f32[4,4]{1,0:T(4,128)S(1)} %multiply_exponential_fusion, pred[512,768]{0,1:T(8,128)(4,1)S(1)} %fusion.24, ...), kind=kOutput, calls=%fused_computation.25 | convolution fusion | flops 845283328 | bytes 28639296 | tf_op jit(solution)/shard_map/kgrs,skd->rkgd/dot_general | solution.py:77
  76.0 3.8 convolution_convert_fusion
  79.9 0.5 all-gather.3.cloned.1.call-update
  80.4 0.5 all-gather.5.cloned.1.call-update
  81.2 24.2 %all-reduce.3.cloned.1.call-done = bf16[512,2048]{1,0:T(8,128)(2,1)} async-done(((bf16[512,2048]{1,0:T(8,128)(2,1)}), bf16[512,2048]{1,0:T(8,128)(2,1)}) %all-reduce.3.cloned.1.call-update) | async-done | bytes 2097168 | tf_op jit(solution)/shard_map/psum | solution.py:88
  105.4 2.4 fusion.7
  107.8 170.2 %all-gather.3.cloned.1.call-done = bf16[2048,4096]{1,0:T(8,128)(2,1)} async-done(((bf16[128,4096]{1,0:T(8,128)(2,1)}), bf16[2048,4096]{1,0:T(8,128)(2,1)}) %all-gather.3.cloned.1.call-update) | async-done | bytes 16777232 | tf_op jit(solution)/shard_map/all_gather | solution.py:30
  278.0 249.7 %all-gather.5.cloned.1.call-done = bf16[4096,2048]{1,0:T(8,128)(2,1)} async-done(((bf16[4096,128]{1,0:T(8,128)(2,1)}), bf16[4096,2048]{1,0:T(8,128)(2,1)}) %all-gather.5.cloned.1.call-update) | async-done | bytes 16777232 | tf_op jit(solution)/shard_map/all_gather | solution.py:34
  527.7 29.8 %convolution_convert_fusion.1 = bf16[512,2048]{1,0:T(8,128)(2,1)} fusion(bf16[4096,2048]{1,0:T(8,128)(2,1)} %all-gather.5.cloned.1.call-done, bf16[2048,4096]{1,0:T(8,128)(2,1)} %all-gather.3.cloned.1.call-done, f32[2048]{0:T(1024)S(1)} %copy-done.3, f32[512]{0:T(512)S(1)} %add_rsqrt_fusion.2, bf16[512,2048]{1,0:T(8,128)(2,1)} %all-reduce.3.cloned.1.call-done, ...), kind=kOutput, calls=%fused_computation.18 | convolution fusion | flops 17195597824 | bytes 39856128 | tf_op jit(solution)/shard_map/dot_general | solution.py:33
  557.6 19.6 %all-reduce.5.cloned.1.call-done = bf16[512,2048]{1,0:T(8,128)(2,1)} async-done(((bf16[512,2048]{1,0:T(8,128)(2,1)}), bf16[512,2048]{1,0:T(8,128)(2,1)}) %all-reduce.5.cloned.1.call-update) | async-done | bytes 2097168 | tf_op jit(solution)/shard_map/psum | solution.py:94
  577.2 4.8 fusion.10
  (32 shorter events, 1.3 us)
Async XLA Ops:
  7.4 26.6 %copy-start.1 = (bf16[512,256]{1,0:T(8,128)(2,1)S(1)}, bf16[512,256]{1,0:T(8,128)(2,1)}, u32[]{:S(2)}) copy-start(bf16[512,256]{1,0:T(8,128)(2,1)} %param.15) | copy-start | bytes 786436
  7.4 98.0 %all-reduce.3.cloned.1.call-start = ((), (), s32[]{:S(2)}) async-start(), calls=%async_computation | async-start | bytes 4194304 | tf_op jit(solution)/shard_map/psum | solution.py:88
  8.6 26.3 %collective-permute-start.2 = (bf16[128]{0:T(256)(128)(2,1)}, bf16[128]{0:T(256)(128)(2,1)}, u32[]{:S(2)}, u32[]{:S(2)}) collective-permute-start(bf16[128]{0:T(256)(128)(2,1)} %get-tuple-element.9), channel_id=1, source_target_pairs={{0,2},{2,4},{4,6},{6,8},{8,10},{10,12},{12,14},{14,16},{16,18},{18... | collective-permute-start | bytes 776 | tf_op jit(solution)/shard_map/ppermute | solution.py:17
  14.1 22.2 %collective-permute-start.3 = (bf16[128]{0:T(256)(128)(2,1)}, bf16[128]{0:T(256)(128)(2,1)}, u32[]{:S(2)}, u32[]{:S(2)}) collective-permute-start(bf16[128]{0:T(256)(128)(2,1)} %get-tuple-element.10), channel_id=1, source_target_pairs={{2,0},{4,2},{6,4},{8,6},{10,8},{12,10},{14,12},{16,14},{18,16},{20... | collective-permute-start | bytes 776 | tf_op jit(solution)/shard_map/ppermute | solution.py:18
  18.0 20.8 %collective-permute-start.4 = (bf16[128,4,64]{0,2,1:T(8,128)(2,1)}, bf16[128,4,64]{0,2,1:T(8,128)(2,1)}, u32[]{:S(2)}, u32[]{:S(2)}) collective-permute-start(bf16[128,4,64]{0,2,1:T(8,128)(2,1)} %get-tuple-element.7), channel_id=1, source_target_pairs={{0,2},{2,4},{4,6},{6,8},{8,10},{10,12},{12,14},{14,16},{16,18},{18... | collective-permute-start | bytes 196616 | tf_op jit(solution)/shard_map/ppermute | solution.py:17
  23.1 15.6 %collective-permute-start.5 = (bf16[128,4,64]{0,2,1:T(8,128)(2,1)}, bf16[128,4,64]{0,2,1:T(8,128)(2,1)}, u32[]{:S(2)}, u32[]{:S(2)}) collective-permute-start(bf16[128,4,64]{0,2,1:T(8,128)(2,1)} %get-tuple-element.8), channel_id=1, source_target_pairs={{2,0},{4,2},{6,4},{8,6},{10,8},{12,10},{14,12},{16,14},{18,16},{20... | collective-permute-start | bytes 196616 | tf_op jit(solution)/shard_map/ppermute | solution.py:18
  25.4 38.0 %collective-permute-start = (bf16[128,4,64]{0,2,1:T(8,128)(2,1)S(1)}, bf16[128,4,64]{0,2,1:T(8,128)(2,1)}, u32[]{:S(2)}, u32[]{:S(2)}) collective-permute-start(bf16[128,4,64]{0,2,1:T(8,128)(2,1)S(1)} %bitcast.52), channel_id=1, source_target_pairs={{0,2},{2,4},{4,6},{6,8},{8,10},{10,12},{12,14},{14,16},{16,18},{18... | collective-permute-start | bytes 196616 | tf_op jit(solution)/shard_map/ppermute | solution.py:17
  35.0 28.5 %collective-permute-start.1 = (bf16[128,4,64]{0,2,1:T(8,128)(2,1)S(1)}, bf16[128,4,64]{0,2,1:T(8,128)(2,1)S(1)}, u32[]{:S(2)}, u32[]{:S(2)}) collective-permute-start(bf16[128,4,64]{0,2,1:T(8,128)(2,1)S(1)} %bitcast.53), channel_id=1, source_target_pairs={{2,0},{4,2},{6,4},{8,6},{10,8},{12,10},{14,12},{16,14},{18,16},{20... | collective-permute-start | bytes 196616 | tf_op jit(solution)/shard_map/ppermute | solution.py:18
  63.5 12.5 %copy-start.2 = (bf16[1024,2048]{1,0:T(8,128)(2,1)S(1)}, bf16[1024,2048]{1,0:T(8,128)(2,1)}, u32[]{:S(2)}) copy-start(bf16[1024,2048]{1,0:T(8,128)(2,1)} %param.20) | copy-start | bytes 12582916
  79.8 25.6 %copy-start = (bf16[512,2048]{1,0:T(8,128)(2,1)S(1)}, bf16[512,2048]{1,0:T(8,128)(2,1)}, u32[]{:S(2)}) copy-start(bf16[512,2048]{1,0:T(8,128)(2,1)} %param.12) | copy-start | bytes 6291460
  79.8 447.9 %copy-start.3 = (f32[2048]{0:T(1024)S(1)}, f32[2048]{0:T(1024)}, u32[]{:S(2)}) copy-start(f32[2048]{0:T(1024)} %param.21) | copy-start | bytes 24580
  79.8 198.2 %all-gather.3.cloned.1.call-start = ((), (), s32[]{:S(2)}) async-start(), calls=%async_computation.1 | async-start | bytes 17825792 | tf_op jit(solution)/shard_map/all_gather | solution.py:30
  80.4 447.3 %all-gather.5.cloned.1.call-start = ((), (), s32[]{:S(2)}) async-start(), calls=%async_computation.2 | async-start | bytes 17825792 | tf_op jit(solution)/shard_map/all_gather | solution.py:34
  81.0 496.2 %all-reduce.5.cloned.1.call-start = ((), (), s32[]{:S(2)}) async-start(), calls=%async_computation.3 | async-start | bytes 4194304 | tf_op jit(solution)/shard_map/psum | solution.py:94
Sparse Core Ops, SparseCore 0:
  79.9 25.4 all-reduce.2
  557.7 19.4 all-reduce.4
Sparse Core Ops, SparseCore 1:
  83.1 194.9 all-gather.2
  280.6 247.1 all-gather.4
where the time goes:
time: 590 us; the launch traced here: 589 us
  waiting for transfers between devices  465 us (79%)
  matrix products  58.5 us (10%)
  other arithmetic  25.2 us (4%)
  starting transfers between devices  19.9 us (3%)
  between operations  15 us (3%)
    all_gather x1, waiting for transfers between devices, mixer_partial(): lax.all_gather(w_down, 'sp', axis=1, tiled=True)  250 us
    all_gather x1, waiting for transfers between devices, mixer_partial(): lax.all_gather(w_up, 'sp', axis=0, tiled=True)  170 us
    dot_general x1, matrix products, mixer_partial(): jnp.dot(active, lax.all_gather(w_down, 'sp', axis=1, tiled=True), preferr...  29.8 us
    psum x1, waiting for transfers between devices, shards(): lax.psum(jnp.dot(attended, w_out, preferred_element_type=jnp.float32).ast...  24.2 us
    psum x1, waiting for transfers between devices, shards(): lax.psum(partial_sum.astype(jnp.bfloat16), 'tp').astype(jnp.float32)  19.6 us
    ppermute x3, starting transfers between devices, extended(): before = lax.ppermute(last, axis, up)  15.8 us
    dot_general x1, matrix products, shards(): jnp.einsum('kgrs,skd->rkgd', weights.astype(jnp.bfloat16), near_values, p...  12.5 us
    dot_general x1, matrix products, shards(): jnp.einsum('rkgd,skd->kgrs', qnorm, near_keys, preferred_element_type=jnp...  12.5 us
  transfers between devices with their start and end apart: 10, of which 4 were waited for; matrix products, arithmetic and copies ran while one was open for 6% of the time, Pallas kernels for 0%

commit v1 on v0

--- a/solution.py
+++ b/solution.py
@@ -31,7 +31,9 @@
     )
     active = jnp.square(jax.nn.relu(upward)).astype(jnp.bfloat16)
     return jnp.dot(
-        active, lax.all_gather(w_down, "sp", axis=1, tiled=True), preferred_element_type=jnp.float32
+        active,
+        jnp.concatenate(lax.all_gather(w_down, "sp"), axis=1),
+        preferred_element_type=jnp.float32,
     )
 
 

time: 590 us -> 527 us (0.89)
  waiting for transfers between devices: 465 us -> 385 us
  local copies, waits for them, and re-layouts: 5.81 us -> 27.1 us
    all_gather x1, waiting for transfers between devices: 250 us -> 170 us  [mixer_partial(): lax.all_gather(w_down, 'sp')]
    reshape x0 -> x1, local copies, waits for them, and re-layouts: none -> 21.3 us  [mixer_partial(): jnp.concatenate(lax.all_gather(w_down, 'sp'), axis=1)]
  transfers between devices with their start and end apart: 10 -> 10, of which waited for: 4 -> 4; matrix products, arithmetic and copies ran while one was open for 6% -> 11% of each run, Pallas kernels for 0% -> 0%
where the time goes in v1:
time: 527 us; the launch traced here: 525 us
  waiting for transfers between devices  385 us (73%)
  matrix products  52.7 us (10%)
  local copies, waits for them, and re-layouts  27.1 us (5%)
  other arithmetic  25.2 us (5%)
  starting transfers between devices  19.9 us (4%)
  between operations  15 us (3%)
    all_gather x1, waiting for transfers between devices, mixer_partial(): lax.all_gather(w_up, 'sp', axis=0, tiled=True)  170 us
    all_gather x1, waiting for transfers between devices, mixer_partial(): lax.all_gather(w_down, 'sp')  170 us
    psum x1, waiting for transfers between devices, shards(): lax.psum(jnp.dot(attended, w_out, preferred_element_type=jnp.float32).ast...  24.2 us
    dot_general x1, matrix products, mixer_partial(): jnp.dot(active, jnp.concatenate(lax.all_gather(w_down, 'sp'), axis=1), pr...  24 us
    reshape x1, local copies, waits for them, and re-layouts, mixer_partial(): jnp.concatenate(lax.all_gather(w_down, 'sp'), axis=1)  21.3 us
    psum x1, waiting for transfers between devices, shards(): lax.psum(partial_sum.astype(jnp.bfloat16), 'tp').astype(jnp.float32)  19.6 us
    ppermute x3, starting transfers between devices, extended(): before = lax.ppermute(last, axis, up)  15.8 us
    dot_general x1, matrix products, shards(): jnp.einsum('kgrs,skd->rkgd', weights.astype(jnp.bfloat16), near_values, p...  12.5 us
  transfers between devices with their start and end apart: 10, of which 4 were waited for; matrix products, arithmetic and copies ran while one was open for 11% of the time, Pallas kernels for 0%

profile of v1, /device:TPU:0, one launch (start us, length us, event | category | flops | bytes accessed | tf_op | source)
XLA Modules:
  0.0 525.4 jit_solution(11413519610624904754)
XLA Ops:
  7.4 0.7 convert_element_type.69
  8.1 0.5 fusion.50
  8.6 5.4 %collective-permute-start.2 = (bf16[128]{0:T(256)(128)(2,1)}, bf16[128]{0:T(256)(128)(2,1)}, u32[]{:S(2)}, u32[]{:S(2)}) collective-permute-start(bf16[128]{0:T(256)(128)(2,1)} %get-tuple-element.9), channel_id=1, source_target_pairs={{0,2},{2,4},{4,6},{6,8},{8,10},{10,12},{12,14},{14,16},{16,18},{18... | collective-permute-start | bytes 776 | tf_op jit(solution)/shard_map/ppermute | solution.py:17
  14.1 1.3 collective-permute-start.3
  15.4 1.1 copy.28
  16.5 0.8 multiply_convert_fusion.1
  17.3 0.7 fusion.49
  18.0 5.2 collective-permute-start.4
  23.1 1.3 collective-permute-start.5
  24.4 0.9 fusion.48
  25.4 5.2 collective-permute-start
  30.6 0.6 fusion.41
  31.2 1.5 copy.29
  33.0 0.6 add_rsqrt_fusion
  34.1 0.7 max.24
  35.0 1.3 collective-permute-start.1
  36.3 0.7 pad_maximum_fusion
  37.0 1.8 fusion.28
  38.8 12.5 %fusion.3 = (f32[4,4,512]{2,1,0:T(4,128)S(1)}, f32[4,768,512,4]{2,1,3,0:T(8,128)}) fusion(f32[512,768]{0,1:T(8,128)S(1)} %fusion.24, f32[4,4]{1,0:T(4,128)S(1)} %multiply_exponential_fusion, pred[512,768]{0,1:T(8,128)(4,1)S(1)} %fusion.28, bf16[512,4,4,64]{0,3,2,1:T(8,128)(2,1)S(1)} %bitcast.51, f32[64]{0:T(128)} %param.17, f32[512,4,4]{0,2,1:T(4,128)} %add_rsqrt_fusion, ...), kind=kOutput, calls=%fused_computation.5 | convolution fusion | flops 840032256 | bytes 28639552 | tf_op jit(solution)/shard_map/rkgd,skd->kgrs/dot_general | solution.py:71
  51.3 12.1 %fusion.1 = f32[4,4,512]{2,1,0:T(4,128)S(1)} fusion(f32[4,768,512,4]{2,1,3,0:T(8,128)} %get-tuple-element.12, f32[4,4,512]{2,1,0:T(4,128)S(1)} %broadcast_maximum_fusion, f32[512,768]{0,1:T(8,128)S(1)} %fusion.24, f32[4,4]{1,0:T(4,128)S(1)} %multiply_exponential_fusion, pred[512,768]{0,1:T(8,128)(4,1)S(1)} %fusion.28), kind=kLoop, calls=%fused_computation.3 | loop fusion | flops 37740544 | bytes 27197504 | tf_op jit(solution)/shard_map/reduce_sum | solution.py:78
  63.5 12.5 %fusion.17 = bf16[512,4,4,64]{0,3,2,1:T(8,128)(2,1)S(1)} fusion(f32[4,768,512,4]{2,1,3,0:T(8,128)} %get-tuple-element.12, f32[4,4,512]{2,1,0:T(4,128)S(1)} %broadcast_maximum_fusion, f32[512,768]{0,1:T(8,128)S(1)} %fusion.24, f32[4,4]{1,0:T(4,128)S(1)} %multiply_exponential_fusion, pred[512,768]{0,1:T(8,128)(4,1)S(1)} %fusion.28, ...), kind=kOutput, calls=%fused_computation.25 | convolution fusion | flops 845283328 | bytes 28639296 | tf_op jit(solution)/shard_map/kgrs,skd->rkgd/dot_general | solution.py:79
  76.0 3.8 convolution_convert_fusion
  79.8 0.5 all-gather.6.cloned.1.call-update
  80.4 0.5 all-gather.4.cloned.1.call-update
  81.2 24.2 %all-reduce.3.cloned.1.call-done = bf16[512,2048]{1,0:T(8,128)(2,1)} async-done(((bf16[512,2048]{1,0:T(8,128)(2,1)}), bf16[512,2048]{1,0:T(8,128)(2,1)}) %all-reduce.3.cloned.1.call-update) | async-done | bytes 2097168 | tf_op jit(solution)/shard_map/psum | solution.py:90
  105.4 2.4 fusion.7
  107.8 170.2 %all-gather.6.cloned.1.call-done = bf16[65536,128]{1,0:T(8,128)(2,1)} async-done(((bf16[4096,128]{1,0:T(8,128)(2,1)}), bf16[65536,128]{1,0:T(8,128)(2,1)}) %all-gather.6.cloned.1.call-update) | async-done | bytes 16777232 | tf_op jit(solution)/shard_map/all_gather | solution.py:35
  278.0 21.3 %copy.31 = bf16[4096,16,128]{0,2,1:T(8,128)(2,1)} copy(bf16[4096,16,128]{2,0,1:T(8,128)(2,1)} %bitcast.49) | data formatting | bytes 33554432 | tf_op jit(solution)/shard_map/reshape | solution.py:35
  299.3 170.3 %all-gather.4.cloned.1.call-done = bf16[2048,4096]{1,0:T(8,128)(2,1)} async-done(((bf16[128,4096]{1,0:T(8,128)(2,1)}), bf16[2048,4096]{1,0:T(8,128)(2,1)}) %all-gather.4.cloned.1.call-update) | async-done | bytes 16777232 | tf_op jit(solution)/shard_map/all_gather | solution.py:30
  469.6 24.0 %convolution_convert_fusion.1 = bf16[512,2048]{1,0:T(8,128)(2,1)} fusion(bf16[4096,2048]{0,1:T(8,128)(2,1)} %bitcast.50, bf16[2048,4096]{1,0:T(8,128)(2,1)} %all-gather.4.cloned.1.call-done, f32[2048]{0:T(1024)S(1)} %copy-done.3, f32[512]{0:T(512)S(1)} %add_rsqrt_fusion.2, bf16[512,2048]{1,0:T(8,128)(2,1)} %all-reduce.3.cloned.1.call-done, ...), kind=kOutput, calls=%fused_computation.18 | convolution fusion | flops 17195597824 | bytes 39856128 | tf_op jit(solution)/shard_map/dot_general | solution.py:33
  493.6 19.6 %all-reduce.5.cloned.1.call-done = bf16[512,2048]{1,0:T(8,128)(2,1)} async-done(((bf16[512,2048]{1,0:T(8,128)(2,1)}), bf16[512,2048]{1,0:T(8,128)(2,1)}) %all-reduce.5.cloned.1.call-update) | async-done | bytes 2097168 | tf_op jit(solution)/shard_map/psum | solution.py:96
  513.2 4.8 fusion.10
  (33 shorter events, 1.6 us)
Async XLA Ops:
  7.4 26.6 %copy-start.1 = (bf16[512,256]{1,0:T(8,128)(2,1)S(1)}, bf16[512,256]{1,0:T(8,128)(2,1)}, u32[]{:S(2)}) copy-start(bf16[512,256]{1,0:T(8,128)(2,1)} %param.15) | copy-start | bytes 786436
  7.4 98.0 %all-reduce.3.cloned.1.call-start = ((), (), s32[]{:S(2)}) async-start(), calls=%async_computation | async-start | bytes 4194304 | tf_op jit(solution)/shard_map/psum | solution.py:90
  8.6 26.3 %collective-permute-start.2 = (bf16[128]{0:T(256)(128)(2,1)}, bf16[128]{0:T(256)(128)(2,1)}, u32[]{:S(2)}, u32[]{:S(2)}) collective-permute-start(bf16[128]{0:T(256)(128)(2,1)} %get-tuple-element.9), channel_id=1, source_target_pairs={{0,2},{2,4},{4,6},{6,8},{8,10},{10,12},{12,14},{14,16},{16,18},{18... | collective-permute-start | bytes 776 | tf_op jit(solution)/shard_map/ppermute | solution.py:17
  14.1 22.2 %collective-permute-start.3 = (bf16[128]{0:T(256)(128)(2,1)}, bf16[128]{0:T(256)(128)(2,1)}, u32[]{:S(2)}, u32[]{:S(2)}) collective-permute-start(bf16[128]{0:T(256)(128)(2,1)} %get-tuple-element.10), channel_id=1, source_target_pairs={{2,0},{4,2},{6,4},{8,6},{10,8},{12,10},{14,12},{16,14},{18,16},{20... | collective-permute-start | bytes 776 | tf_op jit(solution)/shard_map/ppermute | solution.py:18
  18.0 20.8 %collective-permute-start.4 = (bf16[128,4,64]{0,2,1:T(8,128)(2,1)}, bf16[128,4,64]{0,2,1:T(8,128)(2,1)}, u32[]{:S(2)}, u32[]{:S(2)}) collective-permute-start(bf16[128,4,64]{0,2,1:T(8,128)(2,1)} %get-tuple-element.7), channel_id=1, source_target_pairs={{0,2},{2,4},{4,6},{6,8},{8,10},{10,12},{12,14},{14,16},{16,18},{18... | collective-permute-start | bytes 196616 | tf_op jit(solution)/shard_map/ppermute | solution.py:17
  23.1 15.6 %collective-permute-start.5 = (bf16[128,4,64]{0,2,1:T(8,128)(2,1)}, bf16[128,4,64]{0,2,1:T(8,128)(2,1)}, u32[]{:S(2)}, u32[]{:S(2)}) collective-permute-start(bf16[128,4,64]{0,2,1:T(8,128)(2,1)} %get-tuple-element.8), channel_id=1, source_target_pairs={{2,0},{4,2},{6,4},{8,6},{10,8},{12,10},{14,12},{16,14},{18,16},{20... | collective-permute-start | bytes 196616 | tf_op jit(solution)/shard_map/ppermute | solution.py:18
  25.4 38.0 %collective-permute-start = (bf16[128,4,64]{0,2,1:T(8,128)(2,1)S(1)}, bf16[128,4,64]{0,2,1:T(8,128)(2,1)}, u32[]{:S(2)}, u32[]{:S(2)}) collective-permute-start(bf16[128,4,64]{0,2,1:T(8,128)(2,1)S(1)} %bitcast.53), channel_id=1, source_target_pairs={{0,2},{2,4},{4,6},{6,8},{8,10},{10,12},{12,14},{14,16},{16,18},{18... | collective-permute-start | bytes 196616 | tf_op jit(solution)/shard_map/ppermute | solution.py:17
  35.0 28.5 %collective-permute-start.1 = (bf16[128,4,64]{0,2,1:T(8,128)(2,1)S(1)}, bf16[128,4,64]{0,2,1:T(8,128)(2,1)S(1)}, u32[]{:S(2)}, u32[]{:S(2)}) collective-permute-start(bf16[128,4,64]{0,2,1:T(8,128)(2,1)S(1)} %bitcast.54), channel_id=1, source_target_pairs={{2,0},{4,2},{6,4},{8,6},{10,8},{12,10},{14,12},{16,14},{18,16},{20... | collective-permute-start | bytes 196616 | tf_op jit(solution)/shard_map/ppermute | solution.py:18
  63.5 12.5 %copy-start.2 = (bf16[1024,2048]{1,0:T(8,128)(2,1)S(1)}, bf16[1024,2048]{1,0:T(8,128)(2,1)}, u32[]{:S(2)}) copy-start(bf16[1024,2048]{1,0:T(8,128)(2,1)} %param.20) | copy-start | bytes 12582916
  79.8 25.6 %copy-start = (bf16[512,2048]{1,0:T(8,128)(2,1)S(1)}, bf16[512,2048]{1,0:T(8,128)(2,1)}, u32[]{:S(2)}) copy-start(bf16[512,2048]{1,0:T(8,128)(2,1)} %param.12) | copy-start | bytes 6291460
  79.8 198.2 %all-gather.6.cloned.1.call-start = ((), (), s32[]{:S(2)}) async-start(), calls=%async_computation.3 | async-start | bytes 17825792 | tf_op jit(solution)/shard_map/all_gather | solution.py:35
  80.4 389.2 %all-gather.4.cloned.1.call-start = ((), (), s32[]{:S(2)}) async-start(), calls=%async_computation.1 | async-start | bytes 17825792 | tf_op jit(solution)/shard_map/all_gather | solution.py:30
  81.0 432.3 %all-reduce.5.cloned.1.call-start = ((), (), s32[]{:S(2)}) async-start(), calls=%async_computation.2 | async-start | bytes 4194304 | tf_op jit(solution)/shard_map/psum | solution.py:96
  278.0 191.6 %copy-start.3 = (f32[2048]{0:T(1024)S(1)}, f32[2048]{0:T(1024)}, u32[]{:S(2)}) copy-start(f32[2048]{0:T(1024)} %param.21) | copy-start | bytes 24580
Sparse Core Ops, SparseCore 0:
  79.9 25.4 all-reduce.2
  493.7 19.4 all-reduce.4
Sparse Core Ops, SparseCore 1:
  83.0 194.9 all-gather.5
  280.6 188.9 all-gather.3
